TPU v7x, 32 devices: a whole 2x2x4 slice. The times are simulated.
32 devices in a mesh: sp: 8 (over z, y), tp: 4 (over x, core).
Axes of the slice: x: 2, y: 2, z: 4, core: 2. Of those that a mesh axis runs over, the one named last changes fastest.
Arguments:
- queries: bfloat16 [5120, 1024], P('sp', 'tp'), may hold values from -6 to 6
- key_input: bfloat16 [5120, 1024], P('sp', 'tp'), may hold values from -6 to 6
- value_input: bfloat16 [5120, 1024], P('sp', 'tp'), may hold values from -6 to 6
- gate_input: bfloat16 [5120, 1024], P('sp', 'tp'), may hold values from -6 to 6
- log_decay: float32 [8, 5120], P('tp', 'sp'), may hold values from -1.6703125 to 0, as said below
- residual: bfloat16 [5120, 2048], P('sp'), may hold values from -52 to 52
- out_weight: bfloat16 [1024, 2048], P('tp'), may hold values from -0.375 to 0.375
- norm_gain: float32 [2048], replicated, may hold values from 0.3 to 2.7, as said below
- norm_bias: float32 [2048], replicated, may hold values from -1.8 to 1.8
- gate_weight: bfloat16 [2048, 5632], P('sp', 'tp'), may hold values from -0.125 to 0.125
- up_weight: bfloat16 [2048, 5632], P('sp', 'tp'), may hold values from -0.125 to 0.125
- down_weight: bfloat16 [5632, 2048], P('tp', 'sp'), may hold values from -0.078125 to 0.078125
- final_gain: float32 [2048], replicated, may hold values from 0.1 to 1.9
- final_bias: float32 [2048], replicated, may hold values from -1.8 to 1.8
Outputs:
- updated: bfloat16 [5120, 2048], P('sp', 'tp')
Inputs may be any that keep to these rules, and one draw needn't show every extreme that they name: `log_decay`: log-decays, never positive. `norm_gain`: positive gains.
All inputs are finite; a program needn't handle non-finite values.
Results may differ from a plain program's by a relative error of at most 0.023.
Values may be sent and summed in bfloat16 or wider, within the bound.
A program may use at most 128 MiB of HBM per device.

v0:
```python
import jax
import jax.numpy as jnp
from jax import lax
from jax.sharding import PartitionSpec as P

HD = 128
BLOCK = 128
ALPHA = 2.0**0.25
EPS = 1e-05
ROPE_BASE = 10000.0


def prefix(x, axis, combine, identity):
    peers, position = (lax.axis_size(axis), lax.axis_index(axis))
    everything = jax.tree.map(
        lambda part, kind: lax.all_gather(part.astype(kind), axis), x, (jnp.bfloat16, jnp.bfloat16)
    )
    start = jax.tree.map(
        lambda part, zero: jnp.broadcast_to(jnp.asarray(zero, part.dtype), part.shape), x, identity
    )

    def hop(k, before):
        reached = k < position
        new = combine(
            before, jax.tree.map(lambda part, own: part[k].astype(own.dtype), everything, x)
        )
        return jax.tree.map(lambda a, b: jnp.where(reached, a, b), new, before)

    return lax.fori_loop(0, peers, hop, start)


def rotate(values, positions):
    half = values.shape[-1] // 2
    freqs = ROPE_BASE ** (-2.0 * jnp.arange(half, dtype=jnp.float32) / values.shape[-1])
    angles = positions[:, None] * freqs[None, :]
    cosine = jnp.cos(angles)[:, None, :]
    sine = jnp.sin(angles)[:, None, :]
    first = values[..., :half]
    latter_operand = values[..., half:]
    return jnp.concatenate(
        [first * cosine - latter_operand * sine, first * sine + latter_operand * cosine], axis=-1
    )


def head_norm(retained):
    center = retained - jnp.mean(retained, axis=-1, keepdims=True)
    spread = jnp.mean(center * center, axis=-1, keepdims=True)
    return center * lax.rsqrt(spread + EPS)


def combine_states(earlier, later):
    return (earlier[0] * later[0], later[1] + later[0][:, None, None] * earlier[1])


def shards(
    queries,
    key_input,
    value_input,
    gate_input,
    log_decay,
    residual,
    out_weight,
    norm_gain,
    norm_bias,
    gate_weight,
    up_weight,
    down_weight,
    final_gain,
    final_bias,
):
    rows = queries.shape[0]
    heads_here = queries.shape[1] // HD
    blocks = rows // BLOCK
    offset = lax.axis_index("sp") * rows
    positions = (offset + jnp.arange(rows, dtype=jnp.int32)).astype(jnp.float32)
    shaped = (rows, heads_here, HD)
    per_block = (blocks, BLOCK, heads_here, HD)
    turned_q = (
        rotate(queries.astype(jnp.float32).reshape(shaped), positions)
        .astype(jnp.bfloat16)
        .reshape(per_block)
    )
    turned_k = (
        rotate(key_input.astype(jnp.float32).reshape(shaped), positions)
        .astype(jnp.bfloat16)
        .reshape(per_block)
    )
    value_blocks = value_input.reshape(per_block)
    cumul = jnp.cumsum(
        jnp.transpose(log_decay.reshape(heads_here, blocks, BLOCK), (1, 0, 2)), axis=2
    )
    cumul_rows = jnp.transpose(cumul, (0, 2, 1))
    lower = jnp.arange(BLOCK)[:, None] >= jnp.arange(BLOCK)[None, :]
    gaps = cumul[:, :, :, None] - cumul[:, :, None, :]
    damping = jnp.where(lower[None, None], jnp.exp(jnp.minimum(gaps, 0.0)), 0.0)
    scores = jnp.einsum("nihd,njhd->nhij", turned_q, turned_k, preferred_element_type=jnp.float32)
    weights = (scores * damping).astype(jnp.bfloat16)
    inner = jnp.einsum("nhij,njhe->nihe", weights, value_blocks, preferred_element_type=jnp.float32)
    ending = cumul[:, :, -1]
    value_broadened = value_blocks.astype(jnp.float32)
    keyed = turned_k.astype(jnp.float32) * jnp.exp(ending[:, None, :] - cumul_rows)[:, :, :, None]
    fresh = jnp.einsum("njhd,njhe->nhde", keyed, value_broadened, precision=lax.Precision.HIGHEST)

    def advance(state, pieces):
        decay_here, fresh_here = pieces
        return (jnp.exp(decay_here)[:, None, None] * state + fresh_here, state)

    local_state, prefixes = lax.scan(
        advance, jnp.zeros((heads_here, HD, HD), jnp.float32), (ending, fresh)
    )
    before = jnp.cumsum(ending, axis=0) - ending
    device_decay = jnp.exp(jnp.sum(ending, axis=0))
    scanned = prefix(
        (device_decay, local_state),
        "sp",
        combine_states,
        (jnp.ones_like(device_decay), jnp.zeros_like(local_state)),
    )
    entering = prefixes + jnp.exp(before)[:, :, None, None] * scanned[1][None]
    query_wide = turned_q.astype(jnp.float32) * jnp.exp(cumul_rows)[:, :, :, None]
    outer = jnp.einsum("nihd,nhde->nihe", query_wide, entering, precision=lax.Precision.HIGHEST)
    normed = head_norm((inner + outer).reshape(shaped)).reshape(rows, heads_here * HD)
    mixed_heads = (jax.nn.silu(gate_input.astype(jnp.float32)) * normed).astype(jnp.bfloat16)
    partial_value = jnp.dot(mixed_heads, out_weight, preferred_element_type=jnp.float32)
    width = residual.shape[1]
    col_width = width // lax.axis_size("tp")
    col_start = lax.axis_index("tp") * col_width

    def own_columns(array):
        return lax.dynamic_slice_in_dim(array, col_start, col_width, array.ndim - 1)

    mix = lax.psum(partial_value.astype(jnp.bfloat16), "tp")
    leading_sum = ALPHA * residual.astype(jnp.float32) + mix.astype(jnp.float32)
    center = leading_sum - jnp.mean(leading_sum, axis=1, keepdims=True)
    spread = jnp.mean(center * center, axis=1, keepdims=True)
    settled = (center * lax.rsqrt(spread + EPS) * norm_gain + norm_bias).astype(jnp.bfloat16)
    settled_cols = own_columns(settled)

    def add_rows(piece):
        return jnp.dot(settled, piece, preferred_element_type=jnp.float32)

    gate_acts = add_rows(lax.all_gather(gate_weight, "sp", axis=0, tiled=True))
    lifted = add_rows(lax.all_gather(up_weight, "sp", axis=0, tiled=True))
    latent_width = (jax.nn.silu(gate_acts) * lifted).astype(jnp.bfloat16)
    terms = jnp.dot(
        latent_width,
        lax.all_gather(down_weight, "sp", axis=1, tiled=True),
        preferred_element_type=jnp.float32,
    )
    ffn_cols = lax.psum_scatter(terms.astype(jnp.bfloat16), "tp", scatter_dimension=1, tiled=True)
    second_sum = ALPHA * settled_cols.astype(jnp.float32) + ffn_cols.astype(jnp.float32)
    totals_two, squares_two = lax.psum(
        (jnp.sum(second_sum, axis=1), jnp.sum(second_sum * second_sum, axis=1)), "tp"
    )
    average_two = totals_two / width
    spread_two = squares_two / width - average_two * average_two
    scaled_two = (second_sum - average_two[:, None]) * lax.rsqrt(spread_two + EPS)[:, None]
    return (scaled_two * own_columns(final_gain) + own_columns(final_bias)).astype(jnp.bfloat16)


def solution(mesh):
    in_specs = (
        P("sp", "tp"),
        P("sp", "tp"),
        P("sp", "tp"),
        P("sp", "tp"),
        P("tp", "sp"),
        P("sp", None),
        P("tp", None),
        P(),
        P(),
        P("sp", "tp"),
        P("sp", "tp"),
        P("tp", "sp"),
        P(),
        P(),
    )
    out_specs = P("sp", "tp")
    return jax.shard_map(shards, mesh=mesh, in_specs=in_specs, out_specs=out_specs, check_vma=False)
```

profile of v0, /device:TPU:0, one launch (start us, length us, event | category | flops | bytes accessed | tf_op | source)
XLA Modules:
  0.0 434.6 jit_solution(10507391402819925788)
XLA Ops:
  7.5 1.2 copy.65
  8.7 1.1 copy.66
  9.9 0.6 multiply_cosine_fusion
  10.5 0.9 subtract_convert_fusion.1
  11.4 0.2 concatenate.21
  11.6 0.3 copy.49
  11.9 0.2 concatenate.22
  12.1 0.3 copy.50
  12.4 1.5 reduce_window_sum.22
  13.9 0.2 slice_reduce_fusion
  14.1 0.1 copy.53
  14.2 0.1 copy.57
  14.5 1.0 fusion.16
  15.5 3.9 while.29
  15.5 0.7 bitcast_dynamic-update-slice_fusion.3
  16.3 0.7 bitcast_dynamic-update-slice_fusion.3
  17.1 0.7 bitcast_dynamic-update-slice_fusion.3
  17.9 0.7 bitcast_dynamic-update-slice_fusion.3
  18.6 0.7 bitcast_dynamic-update-slice_fusion.3
  19.4 33.0 %all-gather = bf16[16,128,128]{2,1,0:T(8,128)(2,1)S(1)} all-gather(bf16[2,128,128]{2,1,0:T(8,128)(2,1)S(1)} %convert_element_type.101), channel_id=2, replica_groups=mesh['sp'=8,'tp'=4] {'sp'}, dimensions={0}, use_global_device_ids=true | all-gather | bytes 589824 | tf_op jit(solution)/shard_map/all_gather | solution.py:16
  52.5 0.6 dynamic-slice
  53.7 0.2 dynamic-update-slice
  54.0 0.2 reduce_window_sum.23
  54.2 21.5 %all-reduce = bf16[16]{0:T(256)(128)(2,1)S(1)} all-reduce(bf16[16]{0:T(256)(128)(2,1)S(1)} %dynamic-update-slice), channel_id=3, replica_groups=mesh['sp'=8,'tp'=4] {'sp'}, use_global_device_ids=true, to_apply=%add | all-reduce | flops 16 | bytes 64
  75.7 0.1 reshape.213
  75.8 1.0 while.30
  76.2 0.1 fusion.57
  76.3 0.1 fusion.57
  76.4 0.1 fusion.57
  76.6 0.1 fusion.57
  76.8 1.1 concatenate.18
  77.9 0.3 copy.45
  78.2 1.1 concatenate.19
  79.3 0.3 copy.46
  79.6 0.1 copy.58
  79.7 3.5 convolution_bitcast_fusion
  83.1 1.9 fusion.44
  85.1 0.9 copy.60
  86.0 0.1 multiply_reduce_fusion.2
  86.1 0.2 copy.62
  86.3 0.2 copy.61
  86.5 0.8 mul.258
  87.3 0.8 sub.78
  88.2 2.5 convolution_convert_fusion.1
  90.7 0.5 all-gather.6.cloned.1.call-update
  91.3 0.5 all-gather.10.cloned.1.call-update
  91.9 0.5 all-gather.8.cloned.1.call-update
  92.4 0.2 reduce-scatter.2.cloned.1.call-start
  92.6 55.3 %all-reduce.4.cloned.1.call-done = bf16[640,2048]{1,0:T(8,128)(2,1)} async-done(((bf16[640,2048]{1,0:T(8,128)(2,1)}), bf16[640,2048]{1,0:T(8,128)(2,1)}) %all-reduce.4.cloned.1.call-update) | async-done | bytes 2621456 | tf_op jit(solution)/shard_map/psum | solution.py:132
  148.0 3.6 fusion.3
  151.7 0.5 copy-done.2
  152.1 1.3 multiply_reduce_fusion
  153.4 3.0 add_convert_fusion
  156.4 26.3 %all-gather.6.cloned.1.call-done = bf16[2048,1408]{1,0:T(8,128)(2,1)} async-done(((bf16[256,1408]{1,0:T(8,128)(2,1)}), bf16[2048,1408]{1,0:T(8,128)(2,1)}) %all-gather.6.cloned.1.call-update) | async-done | bytes 5767184 | tf_op jit(solution)/shard_map/all_gather | solution.py:142
  182.7 9.4 %fusion.45 = f32[640,1408]{1,0:T(8,128)} fusion(bf16[640,2048]{1,0:T(8,128)(2,1)} %add_convert_fusion, bf16[2048,1408]{1,0:T(8,128)(2,1)} %all-gather.6.cloned.1.call-done), kind=kOutput, calls=%fused_computation.87 | convolution fusion | flops 3690987520 | bytes 11993088 | tf_op jit(solution)/shard_map/dot_general | solution.py:140
  192.2 83.6 %all-gather.10.cloned.1.call-done = bf16[1408,2048]{1,0:T(8,128)(2,1)} async-done(((bf16[1408,256]{1,0:T(8,128)(2,1)}), bf16[1408,2048]{1,0:T(8,128)(2,1)}) %all-gather.10.cloned.1.call-update) | async-done | bytes 5767184 | tf_op jit(solution)/shard_map/all_gather | solution.py:147
  275.7 92.4 %all-gather.8.cloned.1.call-done = bf16[2048,1408]{1,0:T(8,128)(2,1)} async-done(((bf16[256,1408]{1,0:T(8,128)(2,1)}), bf16[2048,1408]{1,0:T(8,128)(2,1)}) %all-gather.8.cloned.1.call-update) | async-done | bytes 5767184 | tf_op jit(solution)/shard_map/all_gather | solution.py:143
  368.1 16.2 %convolution_convert_fusion = bf16[640,2048]{1,0:T(8,128)(2,1)} fusion(bf16[1408,2048]{1,0:T(8,128)(2,1)} %all-gather.10.cloned.1.call-done, bf16[640,2048]{1,0:T(8,128)(2,1)} %add_convert_fusion, bf16[2048,1408]{1,0:T(8,128)(2,1)} %all-gather.8.cloned.1.call-done, f32[640,1408]{1,0:T(8,128)} %fusion.45), kind=kOutput, calls=%fused_computation.14 | convolution fusion | flops 7388692480 | bytes 20381696 | tf_op jit(solution)/shard_map/dot_general | solution.py:145
  384.3 0.8 dynamic_slice.32
  385.1 0.8 dynamic_slice.33
  385.8 31.1 %reduce-scatter.2.cloned.1.call-done = bf16[640,512]{1,0:T(8,128)(2,1)} async-done(((bf16[640,2048]{1,0:T(8,128)(2,1)}), bf16[640,512]{1,0:T(8,128)(2,1)}) %reduce-scatter.2.cloned.1.call-update) | async-done | bytes 655376 | tf_op jit(solution)/shard_map/reduce_scatter | solution.py:150
  417.0 1.7 fusion.7
  418.6 5.9 %all-reduce.1 = (f32[640]{0:T(1024)S(1)}, f32[640]{0:T(1024)S(1)}) all-reduce(f32[640]{0:T(1024)S(1)} %get-tuple-element.182, f32[640]{0:T(1024)S(1)} %get-tuple-element.181), channel_id=1, replica_groups=mesh['sp'=8,'tp'=4] {'tp'}, use_global_device_ids=true, to_apply=%region_16.17 | all-reduce | flops 1280 | bytes 10240 | tf_op jit(solution)/shard_map/psum | solution.py:152
  424.5 2.5 add_convert_fusion.1
  (64 shorter events, 1.3 us)
Async XLA Ops:
  7.4 80.8 %copy-start = (bf16[256,2048]{1,0:T(8,128)(2,1)S(1)}, bf16[256,2048]{1,0:T(8,128)(2,1)}, u32[]{:S(2)}) copy-start(bf16[256,2048]{1,0:T(8,128)(2,1)} %param.24) | copy-start | bytes 3145732
  7.4 5.0 %copy-start.6 = (f32[2,640]{1,0:T(2,128)S(1)}, f32[2,640]{1,0:T(2,128)}, u32[]{:S(2)}) copy-start(f32[2,640]{1,0:T(2,128)} %param.22) | copy-start | bytes 15364
  7.4 7.0 %copy-start.3 = (bf16[640,256]{1,0:T(8,128)(2,1)S(1)}, bf16[640,256]{1,0:T(8,128)(2,1)}, u32[]{:S(2)}) copy-start(bf16[640,256]{1,0:T(8,128)(2,1)} %param.20) | copy-start | bytes 983044
  7.4 140.6 %all-reduce.4.cloned.1.call-start = ((), (), s32[]{:S(2)}) async-start(), calls=%async_computation.1 | async-start | bytes 5242880 | tf_op jit(solution)/shard_map/psum | solution.py:132
  12.1 40.4 %copy-start.8 = (u32[32]{0:T(128)S(1)}, u32[32]{0:T(128)}, u32[]{:S(2)}) copy-start(u32[32]{0:T(128)} %constant.93) | copy-start | bytes 388
  85.1 3.1 copy-start.7
  90.7 92.1 %all-gather.6.cloned.1.call-start = ((), (), s32[]{:S(2)}) async-start(), calls=%async_computation.2 | async-start | bytes 6488064 | tf_op jit(solution)/shard_map/all_gather | solution.py:142
  91.2 184.5 %all-gather.10.cloned.1.call-start = ((), (), s32[]{:S(2)}) async-start(), calls=%async_computation.4 | async-start | bytes 6488064 | tf_op jit(solution)/shard_map/all_gather | solution.py:147
  91.8 276.3 %all-gather.8.cloned.1.call-start = ((), (), s32[]{:S(2)}) async-start(), calls=%async_computation.3 | async-start | bytes 6488064 | tf_op jit(solution)/shard_map/all_gather | solution.py:143
  92.4 324.6 %reduce-scatter.2.cloned.1.call-start = ((), (), s32[]{:S(2)}) async-start(), calls=%async_computation.5 | async-start | bytes 3276800 | tf_op jit(solution)/shard_map/reduce_scatter | solution.py:150
  148.0 3.7 copy-start.1
  148.0 4.2 copy-start.2
  151.6 1.8 copy-start.4
  151.6 1.8 copy-start.5
Sparse Core Ops, SparseCore 0:
  90.8 57.1 all-reduce.3
  384.4 32.4 reduce-scatter.1
Sparse Core Ops, SparseCore 1:
  93.3 89.3 all-gather.5
  184.7 91.0 all-gather.9
  277.8 90.3 all-gather.7
where the time goes:
time: 435 us
  waiting for transfers between devices  290 us (67%)
  blocking collectives  60.4 us (14%)
  matrix products  34.4 us (8%)
  other arithmetic  20.3 us (5%)
  between operations  16 us (4%)
  local copies, waits for them, and re-layouts  12.4 us (3%)
    all_gather x1, waiting for transfers between devices, shards(): lifted = add_rows(lax.all_gather(up_weight, 'sp', axis=0, tiled=True))  92.4 us
    all_gather x1, waiting for transfers between devices, shards(): lax.all_gather(down_weight, 'sp', axis=1, tiled=True)  83.6 us
    psum x1, waiting for transfers between devices, shards(): mix = lax.psum(partial_value.astype(jnp.bfloat16), 'tp')  55.3 us
    all_gather x1, blocking collectives, prefix(): lax.all_gather(part.astype(kind), axis)  33 us
    reduce_scatter x1, waiting for transfers between devices, shards(): lax.psum_scatter(terms.astype(jnp.bfloat16), 'tp', scatter_dimension=1, t...  31.1 us
    all_gather x1, waiting for transfers between devices, shards(): gate_acts = add_rows(lax.all_gather(gate_weight, 'sp', axis=0, tiled=True))  26.3 us
    unnamed x1, blocking collectives  21.5 us
    dot_general x1, matrix products, shards(): jnp.dot(latent_width, lax.all_gather(down_weight, 'sp', axis=1, tiled=Tru...  16.2 us
  transfers between devices with their start and end apart: 5, of which 5 were waited for; matrix products, arithmetic and copies ran while one was open for 4% of the time, Pallas kernels for 0%

commit v1 on v0

--- a/solution.py
+++ b/solution.py
@@ -129,7 +129,7 @@
     def own_columns(array):
         return lax.dynamic_slice_in_dim(array, col_start, col_width, array.ndim - 1)
 
-    mix = lax.psum(partial_value.astype(jnp.bfloat16), "tp")
+    mix = jnp.sum(lax.all_gather(partial_value.astype(jnp.bfloat16), "tp"), axis=0)
     leading_sum = ALPHA * residual.astype(jnp.float32) + mix.astype(jnp.float32)
     center = leading_sum - jnp.mean(leading_sum, axis=1, keepdims=True)
     spread = jnp.mean(center * center, axis=1, keepdims=True)

time: 435 us -> 504 us (1.16)
  waiting for transfers between devices: 290 us -> 352 us
  other arithmetic: 20.3 us -> 29.4 us
    all_gather x0 -> x1, waiting for transfers between devices: none -> 65.3 us  [shards(): lax.all_gather(partial_value.astype(jnp.bfloat16), 'tp')]
    psum x1 -> x0, waiting for transfers between devices: 55.3 us -> none  [shards(): mix = lax.psum(partial_value.astype(jnp.bfloat16), 'tp')]
    all_gather x1, waiting for transfers between devices: 26.3 us -> 76.7 us  [shards(): gate_acts = add_rows(lax.all_gather(gate_weight, 'sp', axis=0, tiled=True))]
    all_gather x1, waiting for transfers between devices: 83.6 us -> 93.2 us  [shards(): lax.all_gather(down_weight, 'sp', axis=1, tiled=True)]
    all_gather x1, waiting for transfers between devices: 92.4 us -> 83.3 us  [shards(): lifted = add_rows(lax.all_gather(up_weight, 'sp', axis=0, tiled=True))]
    reduce_sum x0 -> x1, other arithmetic: none -> 8.83 us  [shards(): jnp.sum(lax.all_gather(partial_value.astype(jnp.bfloat16), 'tp'), axis=0)]
  transfers between devices with their start and end apart: 5 -> 5, of which waited for: 5 -> 5; matrix products, arithmetic and copies ran while one was open for 4% -> 6% of each run, Pallas kernels for 0% -> 0%
where the time goes in v1:
time: 504 us
  waiting for transfers between devices  352 us (70%)
  blocking collectives  60.4 us (12%)
  matrix products  34.7 us (7%)
  other arithmetic  29.4 us (6%)
  between operations  14.1 us (3%)
  local copies, waits for them, and re-layouts  12.6 us (2%)
    all_gather x1, waiting for transfers between devices, shards(): lax.all_gather(down_weight, 'sp', axis=1, tiled=True)  93.2 us
    all_gather x1, waiting for transfers between devices, shards(): lifted = add_rows(lax.all_gather(up_weight, 'sp', axis=0, tiled=True))  83.3 us
    all_gather x1, waiting for transfers between devices, shards(): gate_acts = add_rows(lax.all_gather(gate_weight, 'sp', axis=0, tiled=True))  76.7 us
    all_gather x1, waiting for transfers between devices, shards(): lax.all_gather(partial_value.astype(jnp.bfloat16), 'tp')  65.3 us
    all_gather x1, blocking collectives, prefix(): lax.all_gather(part.astype(kind), axis)  33 us
    reduce_scatter x1, waiting for transfers between devices, shards(): lax.psum_scatter(terms.astype(jnp.bfloat16), 'tp', scatter_dimension=1, t...  31.2 us
    unnamed x1, blocking collectives  21.5 us
    dot_general x1, matrix products, shards(): jnp.dot(latent_width, lax.all_gather(down_weight, 'sp', axis=1, tiled=Tru...  16.4 us
  transfers between devices with their start and end apart: 5, of which 5 were waited for; matrix products, arithmetic and copies ran while one was open for 6% of the time, Pallas kernels for 0%

profile of v1, /device:TPU:0, one launch (start us, length us, event | category | flops | bytes accessed | tf_op | source)
XLA Modules:
  0.0 503.6 jit_solution(12840674363275344268)
XLA Ops:
  6.6 1.2 copy.65
  7.9 1.1 copy.66
  9.0 0.6 multiply_cosine_fusion
  9.7 0.9 subtract_convert_fusion.1
  10.6 0.2 concatenate.21
  10.8 0.3 copy.49
  11.0 0.2 concatenate.22
  11.2 0.3 copy.50
  11.6 1.5 reduce_window_sum.22
  13.1 0.2 slice_reduce_fusion
  13.3 0.1 copy.53
  13.4 0.1 copy.57
  13.7 1.0 fusion.16
  14.6 3.9 while.29
  14.7 0.7 bitcast_dynamic-update-slice_fusion.3
  15.4 0.7 bitcast_dynamic-update-slice_fusion.3
  16.2 0.7 bitcast_dynamic-update-slice_fusion.3
  17.0 0.7 bitcast_dynamic-update-slice_fusion.3
  17.8 0.7 bitcast_dynamic-update-slice_fusion.3
  18.6 33.0 %all-gather = bf16[16,128,128]{2,1,0:T(8,128)(2,1)S(1)} all-gather(bf16[2,128,128]{2,1,0:T(8,128)(2,1)S(1)} %convert_element_type.103), channel_id=2, replica_groups=mesh['sp'=8,'tp'=4] {'sp'}, dimensions={0}, use_global_device_ids=true | all-gather | bytes 589824 | tf_op jit(solution)/shard_map/all_gather | solution.py:16
  51.7 0.6 dynamic-slice
  52.9 0.2 dynamic-update-slice
  53.1 0.2 reduce_window_sum.23
  53.3 21.5 %all-reduce = bf16[16]{0:T(256)(128)(2,1)S(1)} all-reduce(bf16[16]{0:T(256)(128)(2,1)S(1)} %dynamic-update-slice), channel_id=3, replica_groups=mesh['sp'=8,'tp'=4] {'sp'}, use_global_device_ids=true, to_apply=%add | all-reduce | flops 16 | bytes 64
  74.8 0.1 reshape.213
  74.9 1.0 while.30
  75.0 0.1 fusion.57
  75.1 0.1 fusion.57
  75.2 0.1 fusion.57
  75.9 1.1 concatenate.18
  77.1 0.3 copy.45
  77.3 1.1 concatenate.19
  78.5 0.3 copy.46
  78.7 0.1 copy.58
  78.8 3.5 convolution_bitcast_fusion
  82.3 1.9 fusion.44
  84.2 0.9 copy.60
  85.1 0.1 multiply_reduce_fusion.2
  85.3 0.2 copy.62
  85.4 0.2 copy.61
  85.6 0.8 mul.258
  86.5 0.8 sub.78
  87.3 2.6 convolution_convert_fusion.1
  89.9 0.7 all-gather.8.cloned.1.call-update
  90.7 0.7 all-gather.10.cloned.1.call-update
  91.4 0.5 all-gather.12.cloned.1.call-update
  91.9 0.2 reduce-scatter.2.cloned.1.call-start
  92.2 65.3 %all-gather.14.cloned.1.call-done = bf16[2560,2048]{1,0:T(8,128)(2,1)} async-done(((bf16[640,2048]{1,0:T(8,128)(2,1)}), bf16[2560,2048]{1,0:T(8,128)(2,1)}) %all-gather.14.cloned.1.call-update) | async-done | bytes 10485776 | tf_op jit(solution)/shard_map/all_gather | solution.py:132
  157.5 8.8 %reduce_sum.78 = bf16[640,2048]{1,0:T(8,128)(2,1)} reduce(bf16[4,640,2048]{2,1,0:T(8,128)(2,1)} %bitcast.86, bf16[]{:T(256)} %constant.87.clone.1), dimensions={0}, to_apply=%region_9.10 | reduce | flops 3932160 | bytes 13107202 | tf_op jit(solution)/shard_map/reduce_sum | solution.py:132
  166.3 4.0 fusion.3
  170.3 0.7 copy-done.2
  171.0 1.3 multiply_reduce_fusion
  172.3 3.0 add_convert_fusion
  175.3 76.7 %all-gather.8.cloned.1.call-done = bf16[2048,1408]{1,0:T(8,128)(2,1)} async-done(((bf16[256,1408]{1,0:T(8,128)(2,1)}), bf16[2048,1408]{1,0:T(8,128)(2,1)}) %all-gather.8.cloned.1.call-update) | async-done | bytes 5767184 | tf_op jit(solution)/shard_map/all_gather | solution.py:142
  252.0 9.4 %fusion.45 = f32[640,1408]{1,0:T(8,128)} fusion(bf16[640,2048]{1,0:T(8,128)(2,1)} %add_convert_fusion, bf16[2048,1408]{1,0:T(8,128)(2,1)} %all-gather.8.cloned.1.call-done), kind=kOutput, calls=%fused_computation.87 | convolution fusion | flops 3690987520 | bytes 11993088 | tf_op jit(solution)/shard_map/dot_general | solution.py:140
  261.4 83.3 %all-gather.10.cloned.1.call-done = bf16[2048,1408]{1,0:T(8,128)(2,1)} async-done(((bf16[256,1408]{1,0:T(8,128)(2,1)}), bf16[2048,1408]{1,0:T(8,128)(2,1)}) %all-gather.10.cloned.1.call-update) | async-done | bytes 5767184 | tf_op jit(solution)/shard_map/all_gather | solution.py:143
  344.7 93.2 %all-gather.12.cloned.1.call-done = bf16[1408,2048]{1,0:T(8,128)(2,1)} async-done(((bf16[1408,256]{1,0:T(8,128)(2,1)}), bf16[1408,2048]{1,0:T(8,128)(2,1)}) %all-gather.12.cloned.1.call-update) | async-done | bytes 5767184 | tf_op jit(solution)/shard_map/all_gather | solution.py:147
  438.0 16.4 %convolution_convert_fusion = bf16[640,2048]{1,0:T(8,128)(2,1)} fusion(bf16[1408,2048]{1,0:T(8,128)(2,1)} %all-gather.12.cloned.1.call-done, bf16[640,2048]{1,0:T(8,128)(2,1)} %add_convert_fusion, bf16[2048,1408]{1,0:T(8,128)(2,1)} %all-gather.10.cloned.1.call-done, f32[640,1408]{1,0:T(8,128)} %fusion.45), kind=kOutput, calls=%fused_computation.14 | convolution fusion | flops 7388692480 | bytes 20381696 | tf_op jit(solution)/shard_map/dot_general | solution.py:145
  454.4 0.8 dynamic_slice.32
  455.1 0.8 dynamic_slice.33
  455.9 31.2 %reduce-scatter.2.cloned.1.call-done = bf16[640,512]{1,0:T(8,128)(2,1)} async-done(((bf16[640,2048]{1,0:T(8,128)(2,1)}), bf16[640,512]{1,0:T(8,128)(2,1)}) %reduce-scatter.2.cloned.1.call-update) | async-done | bytes 655376 | tf_op jit(solution)/shard_map/reduce_scatter | solution.py:150
  487.0 1.7 fusion.7
  488.7 5.9 %all-reduce.1 = (f32[640]{0:T(1024)S(1)}, f32[640]{0:T(1024)S(1)}) all-reduce(f32[640]{0:T(1024)S(1)} %get-tuple-element.182, f32[640]{0:T(1024)S(1)} %get-tuple-element.181), channel_id=1, replica_groups=mesh['sp'=8,'tp'=4] {'tp'}, use_global_device_ids=true, to_apply=%region_16.17 | all-reduce | flops 1280 | bytes 10240 | tf_op jit(solution)/shard_map/psum | solution.py:152
  494.6 2.5 add_convert_fusion.1
  (65 shorter events, 1.4 us)
Async XLA Ops:
  6.5 80.8 %copy-start = (bf16[256,2048]{1,0:T(8,128)(2,1)S(1)}, bf16[256,2048]{1,0:T(8,128)(2,1)}, u32[]{:S(2)}) copy-start(bf16[256,2048]{1,0:T(8,128)(2,1)} %param.24) | copy-start | bytes 3145732
  6.5 5.0 copy-start.6
  6.5 7.0 %copy-start.3 = (bf16[640,256]{1,0:T(8,128)(2,1)S(1)}, bf16[640,256]{1,0:T(8,128)(2,1)}, u32[]{:S(2)}) copy-start(bf16[640,256]{1,0:T(8,128)(2,1)} %param.20) | copy-start | bytes 983044
  6.5 150.9 %all-gather.14.cloned.1.call-start = ((), (), s32[]{:S(2)}) async-start(), calls=%async_computation.5 | async-start | bytes 13107200 | tf_op jit(solution)/shard_map/all_gather | solution.py:132
  11.2 40.4 %copy-start.8 = (u32[32]{0:T(128)S(1)}, u32[32]{0:T(128)}, u32[]{:S(2)}) copy-start(u32[32]{0:T(128)} %constant.95) | copy-start | bytes 388
  84.2 3.1 copy-start.7
  89.9 162.1 %all-gather.8.cloned.1.call-start = ((), (), s32[]{:S(2)}) async-start(), calls=%async_computation.1 | async-start | bytes 6488064 | tf_op jit(solution)/shard_map/all_gather | solution.py:142
  90.6 254.1 %all-gather.10.cloned.1.call-start = ((), (), s32[]{:S(2)}) async-start(), calls=%async_computation.2 | async-start | bytes 6488064 | tf_op jit(solution)/shard_map/all_gather | solution.py:143
  91.4 346.6 %all-gather.12.cloned.1.call-start = ((), (), s32[]{:S(2)}) async-start(), calls=%async_computation.3 | async-start | bytes 6488064 | tf_op jit(solution)/shard_map/all_gather | solution.py:147
  91.9 395.1 %reduce-scatter.2.cloned.1.call-start = ((), (), s32[]{:S(2)}) async-start(), calls=%async_computation.4 | async-start | bytes 3276800 | tf_op jit(solution)/shard_map/reduce_scatter | solution.py:150
  166.3 4.0 copy-start.1
  166.3 4.7 copy-start.2
  170.3 2.0 copy-start.4
  170.3 2.0 copy-start.5
Sparse Core Ops, SparseCore 0:
  90.0 67.4 all-gather.13
  159.6 92.3 all-gather.7
  254.2 90.4 all-gather.9
  346.6 91.2 all-gather.11
  454.5 32.5 reduce-scatter.1
